TPU v7x, 32 devices: a whole 2x2x4 slice. The times are simulated.
32 devices in a mesh: fs: 16 (over z, y, x), tp: 2 (over core).
Axes of the slice: x: 2, y: 2, z: 4, core: 2. Of those that a mesh axis runs over, the one named last changes fastest.
Arguments:
- late_input: bfloat16 [2048, 2048], P('fs', 'tp'), may hold values from -6 to 6
- up_weight: bfloat16 [2048, 4096], P('tp', 'fs'), may hold values from -0.125 to 0.125
- down_weight: bfloat16 [4096, 2048], P('fs', 'tp'), may hold values from -0.09375 to 0.09375
- early_input: bfloat16 [2048, 2048], P('fs', 'tp'), may hold values from -6 to 6
- early_pre: bfloat16 [2048, 4096], P('fs'), may hold values from -6 to 6
- cotangent: bfloat16 [2048, 2048], P('fs', 'tp'), may hold values from -6 to 6
- up_sum: float32 [2048, 4096], P('tp', 'fs'), may hold values from -24 to 24
- down_sum: float32 [4096, 2048], P('fs', 'tp'), may hold values from -24 to 24
Outputs:
- late_pre: bfloat16 [2048, 4096], P('fs')
- late_out: bfloat16 [2048, 2048], P('fs', 'tp')
- input_grad: bfloat16 [2048, 2048], P('fs', 'tp')
- up_total: float32 [2048, 4096], P('tp', 'fs')
- down_total: float32 [4096, 2048], P('fs', 'tp')
All inputs are finite; a program needn't handle non-finite values.
Results may differ from a plain program's by a relative error of at most 0.025.
Values may be sent and summed in bfloat16 or wider, within the bound.
A program may use at most 128 MiB of HBM per device.

v0:
```python
import jax
import jax.numpy as jnp
from jax import lax
from jax.sharding import PartitionSpec as P


def contract_rows(left, right):
    return lax.dot_general(
        left, right, (((0,), (0,)), ((), ())), preferred_element_type=jnp.float32
    )


def contract_cols(left, right):
    return lax.dot_general(
        left, right, (((1,), (1,)), ((), ())), preferred_element_type=jnp.float32
    )


def body(late_input, up_weight, down_weight, early_input, early_pre, cotangent, up_sum, down_sum):
    up_gathered = lax.all_gather(up_weight, "fs", axis=1, tiled=True)
    down_gathered = lax.all_gather(down_weight, "fs", axis=0, tiled=True)
    pre_terms = jnp.dot(late_input, up_gathered, preferred_element_type=jnp.float32)
    pre_summed = lax.psum(pre_terms.astype(jnp.bfloat16), "tp")
    late_hidden = jnp.square(jax.nn.relu(pre_summed.astype(jnp.float32))).astype(jnp.bfloat16)
    early_float = early_pre.astype(jnp.float32)
    early_hidden = jnp.square(jax.nn.relu(early_float)).astype(jnp.bfloat16)
    late_out = jnp.dot(late_hidden, down_gathered, preferred_element_type=jnp.float32).astype(
        jnp.bfloat16
    )
    grad_terms = contract_cols(cotangent, down_gathered)
    hidden_grad = lax.psum(grad_terms.astype(jnp.bfloat16), "tp").astype(jnp.float32)
    pre_grad = (hidden_grad * 2.0 * jax.nn.relu(early_float)).astype(jnp.bfloat16)
    input_grad = contract_cols(pre_grad, up_gathered).astype(jnp.bfloat16)
    grad_local, hidden_local = (
        lax.all_to_all(pre_grad, "fs", split_axis=1, concat_axis=0, tiled=True),
        lax.all_to_all(early_hidden, "fs", split_axis=1, concat_axis=0, tiled=True),
    )
    rows = grad_local
    up_grad = contract_rows(lax.all_gather(early_input, "fs", axis=0, tiled=True), rows)
    up_total = up_sum + up_grad
    rows = hidden_local
    down_grad = contract_rows(rows, lax.all_gather(cotangent, "fs", axis=0, tiled=True))
    down_total = down_sum + down_grad
    return (pre_summed, late_out, input_grad, up_total, down_total)


def solution(mesh):
    in_specs = (
        P("fs", "tp"),
        P("tp", "fs"),
        P("fs", "tp"),
        P("fs", "tp"),
        P("fs", None),
        P("fs", "tp"),
        P("tp", "fs"),
        P("fs", "tp"),
    )
    out_specs = (P("fs", None), P("fs", "tp"), P("fs", "tp"), P("tp", "fs"), P("fs", "tp"))
    return jax.shard_map(body, mesh=mesh, in_specs=in_specs, out_specs=out_specs, check_vma=False)
```

profile of v0, /device:TPU:0, one launch (start us, length us, event | category | flops | bytes accessed | tf_op | source)
XLA Modules:
  0.0 475.7 jit_solution(18036895991787188094)
XLA Ops:
  7.2 0.7 all-gather.7.cloned.1.call-update
  8.0 0.7 all-gather.5.cloned.1.call-update
  8.7 117.1 %all-gather.7.cloned.1.call-done = bf16[4096,1024]{1,0:T(8,128)(2,1)} async-done(((bf16[256,1024]{1,0:T(8,128)(2,1)}), bf16[4096,1024]{1,0:T(8,128)(2,1)}) %all-gather.7.cloned.1.call-update) | async-done | bytes 8388624 | tf_op jit(solution)/shard_map/all_gather | solution.py:21
  125.8 7.3 %convolution_convert_fusion = bf16[128,4096]{1,0:T(8,128)(2,1)} fusion(bf16[128,1024]{1,0:T(8,128)(2,1)} %param.13, bf16[4096,1024]{1,0:T(8,128)(2,1)} %all-gather.7.cloned.1.call-done), kind=kOutput, calls=%fused_computation | convolution fusion | flops 1074266112 | bytes 9699328 | tf_op jit(solution)/shard_map/dot_general | solution.py:14
  133.2 128.1 %all-gather.5.cloned.1.call-done = bf16[1024,4096]{1,0:T(8,128)(2,1)} async-done(((bf16[1024,256]{1,0:T(8,128)(2,1)}), bf16[1024,4096]{1,0:T(8,128)(2,1)}) %all-gather.5.cloned.1.call-update) | async-done | bytes 8388624 | tf_op jit(solution)/shard_map/all_gather | solution.py:20
  261.2 5.6 %convolution_convert_fusion.1 = bf16[128,4096]{1,0:T(8,128)(2,1)} fusion(bf16[128,1024]{1,0:T(8,128)(2,1)S(1)} %copy-done, bf16[1024,4096]{1,0:T(8,128)(2,1)} %all-gather.5.cloned.1.call-done), kind=kOutput, calls=%fused_computation.1 | convolution fusion | flops 1074266112 | bytes 9699328 | tf_op jit(solution)/shard_map/dot_general | solution.py:22
  266.9 0.5 all-gather.9.cloned.1.call-update
  267.5 0.5 all-gather.11.cloned.1.call-update
  268.0 18.6 %all-reduce.3.cloned.1.call-done = (bf16[128,4096]{1,0:T(8,128)(2,1)}, bf16[128,4096]{1,0:T(8,128)(2,1)}) async-done(((bf16[128,4096]{1,0:T(8,128)(2,1)}, bf16[128,4096]{1,0:T(8,128)(2,1)}), (bf16[128,4096]{1,0:T(8,128)(2,1)}, bf16[128,4096]{1,0:T(8,128)(2,1)})) %all-reduce.3.cloned.1.call-update) | async-done | bytes 2097168 | tf_op jit(solution)/shard_map/psum | solution.py:23
  286.6 1.7 multiply_convert_fusion
  288.4 1.1 copy.24
  289.4 6.8 %all-to-all-start = ((bf16[128,16,256]{2,0,1:T(8,128)(2,1)}), bf16[128,16,256]{2,0,1:T(8,128)(2,1)}, u32[]{:S(2)}, u32[]{:S(2)}) async-start(bf16[128,16,256]{2,0,1:T(8,128)(2,1)} %bitcast.28), calls=%async_computation | async-start | bytes 2097152 | tf_op jit(solution)/shard_map/all_to_all | solution.py:35
  296.3 1.1 copy.23
  297.4 29.2 %all-to-all-done = bf16[128,16,256]{2,0,1:T(8,128)(2,1)} async-done(((bf16[128,16,256]{2,0,1:T(8,128)(2,1)}), bf16[128,16,256]{2,0,1:T(8,128)(2,1)}, u32[]{:S(2)}, u32[]{:S(2)}) %all-to-all-start) | async-done | bytes 1048608 | tf_op jit(solution)/shard_map/all_to_all | solution.py:35
  326.6 6.5 %all-to-all-start.1 = ((bf16[128,16,256]{2,0,1:T(8,128)(2,1)}), bf16[128,16,256]{2,0,1:T(8,128)(2,1)}, u32[]{:S(2)}, u32[]{:S(2)}) async-start(bf16[128,16,256]{2,0,1:T(8,128)(2,1)} %bitcast.27), calls=%async_computation.1 | async-start | bytes 2097152 | tf_op jit(solution)/shard_map/all_to_all | solution.py:36
  333.1 1.3 copy.16
  334.5 7.1 %convolution_convert_fusion.2 = bf16[128,1024]{1,0:T(8,128)(2,1)} fusion(bf16[128,4096]{1,0:T(8,128)(2,1)S(1)} %get-tuple-element.18, bf16[1024,4096]{1,0:T(8,128)(2,1)} %all-gather.5.cloned.1.call-done), kind=kOutput, calls=%fused_computation.9 | convolution fusion | flops 1073872896 | bytes 9699328 | tf_op jit(solution)/shard_map/dot_general | solution.py:14
  341.5 5.4 %convolution_convert_fusion.3 = bf16[128,1024]{1,0:T(8,128)(2,1)} fusion(bf16[4096,1024]{1,0:T(8,128)(2,1)} %all-gather.7.cloned.1.call-done, bf16[128,4096]{1,0:T(8,128)(2,1)S(1)} %copy-done.2), kind=kOutput, calls=%fused_computation.10 | convolution fusion | flops 1075970048 | bytes 9699328 | tf_op jit(solution)/shard_map/dot_general | solution.py:27
  347.0 39.4 %all-gather.9.cloned.1.call-done = bf16[2048,1024]{1,0:T(8,128)(2,1)} async-done(((bf16[128,1024]{1,0:T(8,128)(2,1)}), bf16[2048,1024]{1,0:T(8,128)(2,1)}) %all-gather.9.cloned.1.call-update) | async-done | bytes 4194320 | tf_op jit(solution)/shard_map/all_gather | solution.py:39
  386.4 3.8 fusion
  390.2 1.3 copy.18
  391.5 71.7 %all-gather.11.cloned.1.call-done = bf16[2048,1024]{1,0:T(8,128)(2,1)} async-done(((bf16[128,1024]{1,0:T(8,128)(2,1)}), bf16[2048,1024]{1,0:T(8,128)(2,1)}) %all-gather.11.cloned.1.call-update) | async-done | bytes 4194320 | tf_op jit(solution)/shard_map/all_gather | solution.py:42
  463.2 5.0 %convolution_add_fusion = f32[256,1024]{1,0:T(8,128)} fusion(f32[256,1024]{1,0:T(8,128)} %param.15, bf16[2048,256]{1,0:T(8,128)(2,1)} %bitcast.4, bf16[2048,1024]{1,0:T(8,128)(2,1)} %all-gather.11.cloned.1.call-done), kind=kOutput, calls=%fused_computation.8 | convolution fusion | flops 1074003968 | bytes 7340032 | tf_op jit(solution)/shard_map/dot_general | solution.py:8
  468.2 1.0 copy.27
  (17 shorter events, 0.2 us)
Async XLA Ops:
  7.2 254.1 %copy-start = (bf16[128,1024]{1,0:T(8,128)(2,1)S(1)}, bf16[128,1024]{1,0:T(8,128)(2,1)}, u32[]{:S(2)}) copy-start(bf16[128,1024]{1,0:T(8,128)(2,1)} %param.8) | copy-start | bytes 786436
  7.2 118.6 %all-gather.7.cloned.1.call-start = ((), (), s32[]{:S(2)}) async-start(), calls=%async_computation.3 | async-start | bytes 8912896 | tf_op jit(solution)/shard_map/all_gather | solution.py:21
  7.9 253.3 %all-gather.5.cloned.1.call-start = ((), (), s32[]{:S(2)}) async-start(), calls=%async_computation.2 | async-start | bytes 8912896 | tf_op jit(solution)/shard_map/all_gather | solution.py:20
  8.7 277.9 %all-reduce.3.cloned.1.call-start = ((), (), s32[]{:S(2)}) async-start(), calls=%async_computation.6 | async-start | bytes 4194304 | tf_op jit(solution)/shard_map/psum | solution.py:23
  133.2 153.5 %copy-start.4 = (bf16[128,4096]{1,0:T(8,128)(2,1)S(1)}, bf16[128,4096]{1,0:T(8,128)(2,1)}, u32[]{:S(2)}) copy-start(bf16[128,4096]{1,0:T(8,128)(2,1)} %param.12) | copy-start | bytes 3145732
  266.9 119.5 %all-gather.9.cloned.1.call-start = ((), (), s32[]{:S(2)}) async-start(), calls=%async_computation.4 | async-start | bytes 4456448 | tf_op jit(solution)/shard_map/all_gather | solution.py:39
  267.4 195.7 %all-gather.11.cloned.1.call-start = ((), (), s32[]{:S(2)}) async-start(), calls=%async_computation.5 | async-start | bytes 4456448 | tf_op jit(solution)/shard_map/all_gather | solution.py:42
  288.3 44.8 %copy-start.1 = (f32[1024,256]{1,0:T(8,128)S(1)}, f32[1024,256]{1,0:T(8,128)}, u32[]{:S(2)}) copy-start(f32[1024,256]{1,0:T(8,128)} %param.14) | copy-start | bytes 3145732
  289.4 37.2 %all-to-all-start = ((bf16[128,16,256]{2,0,1:T(8,128)(2,1)}), bf16[128,16,256]{2,0,1:T(8,128)(2,1)}, u32[]{:S(2)}, u32[]{:S(2)}) async-start(bf16[128,16,256]{2,0,1:T(8,128)(2,1)} %bitcast.28), calls=%async_computation | async-start | bytes 2097152 | tf_op jit(solution)/shard_map/all_to_all | solution.py:35
  326.6 136.6 %all-to-all-start.1 = ((bf16[128,16,256]{2,0,1:T(8,128)(2,1)}), bf16[128,16,256]{2,0,1:T(8,128)(2,1)}, u32[]{:S(2)}, u32[]{:S(2)}) async-start(bf16[128,16,256]{2,0,1:T(8,128)(2,1)} %bitcast.27), calls=%async_computation.1 | async-start | bytes 2097152 | tf_op jit(solution)/shard_map/all_to_all | solution.py:36
  334.5 7.1 %copy-start.2 = (bf16[128,4096]{1,0:T(8,128)(2,1)S(1)}, bf16[128,4096]{1,0:T(8,128)(2,1)}, u32[]{:S(2)}) copy-start(bf16[128,4096]{1,0:T(8,128)(2,1)} %get-tuple-element.19) | copy-start | bytes 3145732
  341.5 44.8 %copy-start.3 = (f32[1024,256]{0,1:T(8,128)S(1)}, f32[1024,256]{0,1:T(8,128)}, u32[]{:S(2)}) copy-start(f32[1024,256]{0,1:T(8,128)} %copy.16) | copy-start | bytes 3145732
Sparse Core Ops, SparseCore 0:
  10.8 115.0 all-gather.6
  128.5 132.6 all-gather.4
  267.0 19.5 all-reduce.2
  289.2 97.1 all-gather.8
  389.0 74.1 all-gather.10
where the time goes:
time: 476 us
  waiting for transfers between devices  407 us (86%)
  matrix products  34.3 us (7%)
  between operations  13.8 us (3%)
  starting transfers between devices  13.6 us (3%)
  local copies, waits for them, and re-layouts  5.76 us (1%)
    all_gather x1, waiting for transfers between devices, body(): up_gathered = lax.all_gather(up_weight, 'fs', axis=1, tiled=True)  128 us
    all_gather x1, waiting for transfers between devices, body(): down_gathered = lax.all_gather(down_weight, 'fs', axis=0, tiled=True)  117 us
    all_gather x1, waiting for transfers between devices, body(): lax.all_gather(cotangent, 'fs', axis=0, tiled=True)  71.7 us
    all_gather x1, waiting for transfers between devices, body(): lax.all_gather(early_input, 'fs', axis=0, tiled=True)  39.4 us
    all_to_all x1, waiting for transfers between devices, body(): lax.all_to_all(pre_grad, 'fs', split_axis=1, concat_axis=0, tiled=True)  29.2 us
    psum x1, waiting for transfers between devices, body(): pre_summed = lax.psum(pre_terms.astype(jnp.bfloat16), 'tp')  18.6 us
    dot_general x2, matrix products, contract_cols(): lax.dot_general(left, right, (((1,), (1,)), ((), ())), preferred_element_...  14.4 us
  transfers between devices with their start and end apart: 7, of which 6 were waited for; matrix products, arithmetic and copies ran while one was open for 6% of the time, Pallas kernels for 0%

commit v1 on v0

--- a/solution.py
+++ b/solution.py
@@ -17,7 +17,7 @@
 
 
 def body(late_input, up_weight, down_weight, early_input, early_pre, cotangent, up_sum, down_sum):
-    up_gathered = lax.all_gather(up_weight, "fs", axis=1, tiled=True)
+    up_gathered = jnp.concatenate(lax.all_gather(up_weight, "fs"), axis=1)
     down_gathered = lax.all_gather(down_weight, "fs", axis=0, tiled=True)
     pre_terms = jnp.dot(late_input, up_gathered, preferred_element_type=jnp.float32)
     pre_summed = lax.psum(pre_terms.astype(jnp.bfloat16), "tp")

time: 476 us -> 456 us (0.958)
  waiting for transfers between devices: 407 us -> 374 us
  local copies, waits for them, and re-layouts: 5.76 us -> 18.1 us
    all_gather x1, waiting for transfers between devices: 117 us -> 93.7 us  [body(): down_gathered = lax.all_gather(down_weight, 'fs', axis=0, tiled=True)]
    reshape x0 -> x1, local copies, waits for them, and re-layouts: none -> 12.3 us  [body(): up_gathered = jnp.concatenate(lax.all_gather(up_weight, 'fs'), axis=1)]
    all_gather x1, waiting for transfers between devices: 128 us -> 117 us  [body(): up_gathered = jnp.concatenate(lax.all_gather(up_weight, 'fs'), axis=1)]
  transfers between devices with their start and end apart: 7 -> 7, of which waited for: 6 -> 6; matrix products, arithmetic and copies ran while one was open for 6% -> 9% of each run, Pallas kernels for 0% -> 0%
where the time goes in v1:
time: 456 us; the launch traced here: 455 us
  waiting for transfers between devices  374 us (82%)
  matrix products  34.3 us (8%)
  local copies, waits for them, and re-layouts  18.1 us (4%)
  between operations  13.8 us (3%)
  starting transfers between devices  13.6 us (3%)
    all_gather x1, waiting for transfers between devices, body(): up_gathered = jnp.concatenate(lax.all_gather(up_weight, 'fs'), axis=1)  117 us
    all_gather x1, waiting for transfers between devices, body(): down_gathered = lax.all_gather(down_weight, 'fs', axis=0, tiled=True)  93.7 us
    all_gather x1, waiting for transfers between devices, body(): lax.all_gather(cotangent, 'fs', axis=0, tiled=True)  71.7 us
    all_gather x1, waiting for transfers between devices, body(): lax.all_gather(early_input, 'fs', axis=0, tiled=True)  41 us
    all_to_all x1, waiting for transfers between devices, body(): lax.all_to_all(pre_grad, 'fs', split_axis=1, concat_axis=0, tiled=True)  29.2 us
    psum x1, waiting for transfers between devices, body(): pre_summed = lax.psum(pre_terms.astype(jnp.bfloat16), 'tp')  18.5 us
    dot_general x2, matrix products, contract_cols(): lax.dot_general(left, right, (((1,), (1,)), ((), ())), preferred_element_...  12.7 us
    reshape x1, local copies, waits for them, and re-layouts, body(): up_gathered = jnp.concatenate(lax.all_gather(up_weight, 'fs'), axis=1)  12.3 us
  transfers between devices with their start and end apart: 7, of which 6 were waited for; matrix products, arithmetic and copies ran while one was open for 9% of the time, Pallas kernels for 0%

profile of v1, /device:TPU:0, one launch (start us, length us, event | category | flops | bytes accessed | tf_op | source)
XLA Modules:
  0.0 455.2 jit_solution(17397854329710446833)
XLA Ops:
  7.2 0.7 all-gather.12.cloned.1.call-update
  8.0 0.7 all-gather.6.cloned.1.call-update
  8.7 117.1 %all-gather.12.cloned.1.call-done = bf16[16384,256]{1,0:T(8,128)(2,1)} async-done(((bf16[1024,256]{1,0:T(8,128)(2,1)}), bf16[16384,256]{1,0:T(8,128)(2,1)}) %all-gather.12.cloned.1.call-update) | async-done | bytes 8388624 | tf_op jit(solution)/shard_map/all_gather | solution.py:20
  125.8 12.3 %copy.19 = bf16[1024,16,256]{0,2,1:T(8,128)(2,1)} copy(bf16[1024,16,256]{2,0,1:T(8,128)(2,1)} %bitcast.36) | data formatting | bytes 16777216 | tf_op jit(solution)/shard_map/reshape | solution.py:20
  138.1 7.3 %convolution_convert_fusion.1 = bf16[128,4096]{1,0:T(8,128)(2,1)} fusion(bf16[128,1024]{1,0:T(8,128)(2,1)S(1)} %copy-done, bf16[1024,4096]{0,1:T(8,128)(2,1)} %bitcast.33), kind=kOutput, calls=%fused_computation.1 | convolution fusion | flops 1074266112 | bytes 9699328 | tf_op jit(solution)/shard_map/dot_general | solution.py:22
  145.4 93.7 %all-gather.6.cloned.1.call-done = bf16[4096,1024]{1,0:T(8,128)(2,1)} async-done(((bf16[256,1024]{1,0:T(8,128)(2,1)}), bf16[4096,1024]{1,0:T(8,128)(2,1)}) %all-gather.6.cloned.1.call-update) | async-done | bytes 8388624 | tf_op jit(solution)/shard_map/all_gather | solution.py:21
  239.1 7.2 %convolution_convert_fusion = bf16[128,4096]{1,0:T(8,128)(2,1)} fusion(bf16[128,1024]{1,0:T(8,128)(2,1)S(1)} %copy-done.1, bf16[4096,1024]{1,0:T(8,128)(2,1)} %all-gather.6.cloned.1.call-done), kind=kOutput, calls=%fused_computation | convolution fusion | flops 1074266112 | bytes 9699328 | tf_op jit(solution)/shard_map/dot_general | solution.py:14
  247.0 0.5 all-gather.10.cloned.1.call-update
  247.5 18.5 %all-reduce.3.cloned.1.call-done = (bf16[128,4096]{1,0:T(8,128)(2,1)}, bf16[128,4096]{1,0:T(8,128)(2,1)}) async-done(((bf16[128,4096]{1,0:T(8,128)(2,1)}, bf16[128,4096]{1,0:T(8,128)(2,1)}), (bf16[128,4096]{1,0:T(8,128)(2,1)}, bf16[128,4096]{1,0:T(8,128)(2,1)})) %all-reduce.3.cloned.1.call-update) | async-done | bytes 2097168 | tf_op jit(solution)/shard_map/psum | solution.py:23
  266.1 1.7 multiply_convert_fusion
  267.8 1.1 copy.29
  268.9 6.8 %all-to-all-start = ((bf16[128,16,256]{2,0,1:T(8,128)(2,1)}), bf16[128,16,256]{2,0,1:T(8,128)(2,1)}, u32[]{:S(2)}, u32[]{:S(2)}) async-start(bf16[128,16,256]{2,0,1:T(8,128)(2,1)} %bitcast.32), calls=%async_computation | async-start | bytes 2097152 | tf_op jit(solution)/shard_map/all_to_all | solution.py:35
  275.7 1.1 copy.28
  276.8 29.2 %all-to-all-done = bf16[128,16,256]{2,0,1:T(8,128)(2,1)} async-done(((bf16[128,16,256]{2,0,1:T(8,128)(2,1)}), bf16[128,16,256]{2,0,1:T(8,128)(2,1)}, u32[]{:S(2)}, u32[]{:S(2)}) %all-to-all-start) | async-done | bytes 1048608 | tf_op jit(solution)/shard_map/all_to_all | solution.py:35
  306.1 6.5 %all-to-all-start.1 = ((bf16[128,16,256]{2,0,1:T(8,128)(2,1)}), bf16[128,16,256]{2,0,1:T(8,128)(2,1)}, u32[]{:S(2)}, u32[]{:S(2)}) async-start(bf16[128,16,256]{2,0,1:T(8,128)(2,1)} %bitcast.31), calls=%async_computation.1 | async-start | bytes 2097152 | tf_op jit(solution)/shard_map/all_to_all | solution.py:36
  312.6 1.3 copy.21
  313.9 5.5 %convolution_convert_fusion.2 = bf16[128,1024]{1,0:T(8,128)(2,1)} fusion(bf16[128,4096]{1,0:T(8,128)(2,1)S(1)} %get-tuple-element.23, bf16[1024,4096]{0,1:T(8,128)(2,1)} %bitcast.34), kind=kOutput, calls=%fused_computation.9 | convolution fusion | flops 1073872896 | bytes 9699328 | tf_op jit(solution)/shard_map/dot_general | solution.py:14
  319.4 5.4 %convolution_convert_fusion.3 = bf16[128,1024]{1,0:T(8,128)(2,1)} fusion(bf16[4096,1024]{1,0:T(8,128)(2,1)} %all-gather.6.cloned.1.call-done, bf16[128,4096]{1,0:T(8,128)(2,1)S(1)} %copy-done.3), kind=kOutput, calls=%fused_computation.10 | convolution fusion | flops 1075970048 | bytes 9699328 | tf_op jit(solution)/shard_map/dot_general | solution.py:27
  324.8 41.0 %all-gather.8.cloned.1.call-done = bf16[2048,1024]{1,0:T(8,128)(2,1)} async-done(((bf16[128,1024]{1,0:T(8,128)(2,1)}), bf16[2048,1024]{1,0:T(8,128)(2,1)}) %all-gather.8.cloned.1.call-update) | async-done | bytes 4194320 | tf_op jit(solution)/shard_map/all_gather | solution.py:39
  365.8 3.8 fusion
  369.6 1.3 copy.23
  370.9 71.7 %all-gather.10.cloned.1.call-done = bf16[2048,1024]{1,0:T(8,128)(2,1)} async-done(((bf16[128,1024]{1,0:T(8,128)(2,1)}), bf16[2048,1024]{1,0:T(8,128)(2,1)}) %all-gather.10.cloned.1.call-update) | async-done | bytes 4194320 | tf_op jit(solution)/shard_map/all_gather | solution.py:42
  442.6 5.0 %convolution_add_fusion = f32[256,1024]{1,0:T(8,128)} fusion(f32[256,1024]{1,0:T(8,128)} %param.15, bf16[2048,256]{1,0:T(8,128)(2,1)} %bitcast.7, bf16[2048,1024]{1,0:T(8,128)(2,1)} %all-gather.10.cloned.1.call-done), kind=kOutput, calls=%fused_computation.8 | convolution fusion | flops 1074003968 | bytes 7340032 | tf_op jit(solution)/shard_map/dot_general | solution.py:8
  447.7 1.0 copy.32
  (20 shorter events, 0.8 us)
Async XLA Ops:
  7.2 131.0 %copy-start = (bf16[128,1024]{1,0:T(8,128)(2,1)S(1)}, bf16[128,1024]{1,0:T(8,128)(2,1)}, u32[]{:S(2)}) copy-start(bf16[128,1024]{1,0:T(8,128)(2,1)} %param.8) | copy-start | bytes 786436
  7.2 118.6 %all-gather.12.cloned.1.call-start = ((), (), s32[]{:S(2)}) async-start(), calls=%async_computation.5 | async-start | bytes 8912896 | tf_op jit(solution)/shard_map/all_gather | solution.py:20
  7.9 231.2 %all-gather.6.cloned.1.call-start = ((), (), s32[]{:S(2)}) async-start(), calls=%async_computation.2 | async-start | bytes 8912896 | tf_op jit(solution)/shard_map/all_gather | solution.py:21
  8.7 257.4 %all-reduce.3.cloned.1.call-start = ((), (), s32[]{:S(2)}) async-start(), calls=%async_computation.6 | async-start | bytes 4194304 | tf_op jit(solution)/shard_map/psum | solution.py:23
  138.1 101.0 %copy-start.1 = (bf16[128,1024]{1,0:T(8,128)(2,1)S(1)}, bf16[128,1024]{1,0:T(8,128)(2,1)}, u32[]{:S(2)}) copy-start(bf16[128,1024]{1,0:T(8,128)(2,1)} %param.13) | copy-start | bytes 786436
  145.4 120.6 %copy-start.5 = (bf16[128,4096]{1,0:T(8,128)(2,1)S(1)}, bf16[128,4096]{1,0:T(8,128)(2,1)}, u32[]{:S(2)}) copy-start(bf16[128,4096]{1,0:T(8,128)(2,1)} %param.12) | copy-start | bytes 3145732
  246.3 119.5 %all-gather.8.cloned.1.call-start = ((), (), s32[]{:S(2)}) async-start(), calls=%async_computation.3 | async-start | bytes 4456448 | tf_op jit(solution)/shard_map/all_gather | solution.py:39
  246.9 195.7 %all-gather.10.cloned.1.call-start = ((), (), s32[]{:S(2)}) async-start(), calls=%async_computation.4 | async-start | bytes 4456448 | tf_op jit(solution)/shard_map/all_gather | solution.py:42
  267.8 44.8 %copy-start.2 = (f32[1024,256]{1,0:T(8,128)S(1)}, f32[1024,256]{1,0:T(8,128)}, u32[]{:S(2)}) copy-start(f32[1024,256]{1,0:T(8,128)} %param.14) | copy-start | bytes 3145732
  268.9 37.2 %all-to-all-start = ((bf16[128,16,256]{2,0,1:T(8,128)(2,1)}), bf16[128,16,256]{2,0,1:T(8,128)(2,1)}, u32[]{:S(2)}, u32[]{:S(2)}) async-start(bf16[128,16,256]{2,0,1:T(8,128)(2,1)} %bitcast.32), calls=%async_computation | async-start | bytes 2097152 | tf_op jit(solution)/shard_map/all_to_all | solution.py:35
  306.1 136.6 %all-to-all-start.1 = ((bf16[128,16,256]{2,0,1:T(8,128)(2,1)}), bf16[128,16,256]{2,0,1:T(8,128)(2,1)}, u32[]{:S(2)}, u32[]{:S(2)}) async-start(bf16[128,16,256]{2,0,1:T(8,128)(2,1)} %bitcast.31), calls=%async_computation.1 | async-start | bytes 2097152 | tf_op jit(solution)/shard_map/all_to_all | solution.py:36
  313.9 5.5 %copy-start.3 = (bf16[128,4096]{1,0:T(8,128)(2,1)S(1)}, bf16[128,4096]{1,0:T(8,128)(2,1)}, u32[]{:S(2)}) copy-start(bf16[128,4096]{1,0:T(8,128)(2,1)} %get-tuple-element.24) | copy-start | bytes 3145732
  319.4 46.5 %copy-start.4 = (f32[1024,256]{0,1:T(8,128)S(1)}, f32[1024,256]{0,1:T(8,128)}, u32[]{:S(2)}) copy-start(f32[1024,256]{0,1:T(8,128)} %copy.21) | copy-start | bytes 3145732
Sparse Core Ops, SparseCore 0:
  10.8 115.0 all-gather.11
  128.6 110.4 all-gather.5
  246.5 19.5 all-reduce.2
  268.7 97.1 all-gather.7
  368.4 74.1 all-gather.9
